TPU v7x, 512 devices: a whole 4x8x8 slice. The times are simulated.
512 devices in a mesh: sp: 128 (over z, y, core), tp: 4 (over x).
Axes of the slice: x: 4, y: 8, z: 8, core: 2. Of those that a mesh axis runs over, the one named last changes fastest.
Arguments:
- stream: bfloat16 [32768, 2048], P('sp', 'tp'), may hold values from -6 to 6
- norm_gain: float32 [2, 2048], replicated, may hold values from 0.1 to 1.9
- w_value: bfloat16 [2, 2048, 1024], P(None, 'sp', 'tp'), may hold values from -0.125 to 0.125
- w_gate: bfloat16 [2, 2048, 1024], P(None, 'sp', 'tp'), may hold values from -0.125 to 0.125
- conv_taps: float32 [2, 128, 1024], P(None, None, 'tp'), as said below
- channel_gain: float32 [2, 1024], P(None, 'tp'), may hold values from 0.1 to 1.9
- w_out: bfloat16 [2, 1024, 2048], P(None, 'tp', 'sp'), may hold values from -0.1875 to 0.1875
Outputs:
- result: bfloat16 [32768, 2048], P('sp', 'tp')
Inputs may be any that keep to these rules, and one draw needn't show every extreme that they name: `conv_taps`: taps of each block of 128 consecutive channels share a scale factor of its own.
All inputs are finite; a program needn't handle non-finite values.
Results may differ from a plain program's by a relative error of at most 0.012.
Values may be sent and summed in bfloat16 or wider, within the bound.
No kernel may reach another device: no remote copies, remote signals or barrier semaphores. Data moves between devices by JAX's collectives and lax.ppermute only.
A program may use at most 64 MiB of HBM per device.

v0:
```python
import jax
import jax.numpy as jnp
from jax import lax
from jax.sharding import Mesh
from jax.sharding import PartitionSpec as P

C = 1024
LAYERS = 2
SP = ("sp_0", "sp_1", "sp_2")


def laid_out(parts, dim):
    parts = jnp.moveaxis(parts, 0, dim)
    lengths = parts.shape
    return parts.reshape(*lengths[:dim], lengths[dim] * lengths[dim + 1], *lengths[dim + 2 :])


def sent_to_all(shard, axis):
    copies = jnp.broadcast_to(shard, (lax.axis_size(axis), *shard.shape))
    return lax.all_to_all(copies, axis, split_axis=0, concat_axis=0, tiled=True)


def collect(shard, axis, dim):
    return laid_out(sent_to_all(shard, axis), dim)


def in_one_piece(arrays, axis, dim, along):
    both = jnp.concatenate(arrays, axis=along)
    whole, at, done = (lax.all_gather(both, axis, axis=dim, tiled=True), 0, [])
    for a in arrays:
        done.append(lax.slice_in_dim(whole, at, at + a.shape[along], axis=along))
        at += a.shape[along]
    return tuple(done)


def from_behind(value, axis, steps):
    count = lax.axis_size(axis)
    initial, last = (max(0, -steps), min(count, count - steps))
    return lax.ppermute(value, axis, [(source, source + steps) for source in range(initial, last)])


def of_everyone(shard, axis):
    return sent_to_all(shard, axis).sum(axis=0)


def stacked_from(shard, axes, turns):
    parts = shard[None]
    for k in turns:
        parts = lax.all_gather(parts, axes[k], axis=0, tiled=True)
    held = [lax.axis_size(axes[k]) for k in reversed(turns)]
    parts = parts.reshape(*held, *shard.shape)
    turned = sorted(range(len(turns)), key=lambda place: turns[len(turns) - 1 - place])
    return parts.transpose(*turned, *range(len(turns), parts.ndim)).reshape(-1, *shard.shape)


def gathered_by_axis(shard, axes, turns, dim):
    return laid_out(stacked_from(shard, axes, turns), dim)


def split_up(shard, dim, size):
    lengths = shard.shape
    parts = shard.reshape(*lengths[:dim], size, lengths[dim] // size, *lengths[dim + 1 :])
    return jnp.moveaxis(parts, dim, 0)


def sum_at_owner(shard, axis, dim):
    parts = split_up(shard, dim, lax.axis_size(axis))
    arrived = lax.all_to_all(parts, axis, split_axis=0, concat_axis=0, tiled=True)
    return arrived.astype(jnp.float32).sum(axis=0)


def shards(stream, norm_gain, w_value, w_gate, conv_taps, channel_gain, w_out):
    x = stream
    tokens_here = stream.shape[0]
    local_ch = w_value.shape[2]
    taps = conv_taps.shape[1]
    for layer in range(LAYERS):
        whole = collect(x, "tp", 1).astype(jnp.float32)
        normed = (
            whole
            * lax.rsqrt(jnp.mean(whole * whole, axis=1, keepdims=True) + 1e-06)
            * norm_gain[layer]
        ).astype(jnp.bfloat16)
        value_whole, gate_whole = in_one_piece((w_value[layer], w_gate[layer]), SP, 0, 1)
        value = jnp.dot(normed, value_whole, preferred_element_type=jnp.float32)
        gate = jnp.dot(normed, gate_whole, preferred_element_type=jnp.float32)
        glu = (value * jax.nn.sigmoid(gate)).astype(jnp.bfloat16)
        before = from_behind(glu[tokens_here - taps :], SP, 1)
        padded = jnp.concatenate([before[1:], glu], axis=0).astype(jnp.float32)
        conv = lax.conv_general_dilated(
            padded[None],
            conv_taps[layer][:, None, :],
            (1,),
            "VALID",
            dimension_numbers=("NWC", "WIO", "NWC"),
            feature_group_count=local_ch,
            precision=lax.Precision.HIGHEST,
        )[0]
        mean = of_everyone(jnp.sum(conv, axis=1, keepdims=True), "tp") / C
        centred = conv - mean
        spread = of_everyone(jnp.sum(centred * centred, axis=1, keepdims=True), "tp") / C
        act = jax.nn.silu(centred * lax.rsqrt(spread + 1e-05) * channel_gain[layer]).astype(
            jnp.bfloat16
        )
        out_whole = gathered_by_axis(w_out[layer], (("sp_0", "sp_1"), "sp_2"), (0, 1), 1)
        terms = jnp.dot(act, out_whole, preferred_element_type=jnp.float32)
        branch = sum_at_owner(terms.astype(jnp.bfloat16), "tp", 1)
        x = (x.astype(jnp.float32) + branch).astype(jnp.bfloat16)
    return x


def solution(mesh):
    finer = Mesh(mesh.devices.reshape(8, 8, 2, mesh.shape["tp"]), ("sp_0", "sp_1", "sp_2", "tp"))
    in_specs = (
        P(SP, "tp"),
        P(),
        P(None, SP, "tp"),
        P(None, SP, "tp"),
        P(None, None, "tp"),
        P(None, "tp"),
        P(None, "tp", SP),
    )
    out_specs = P(SP, "tp")
    return jax.shard_map(
        shards, mesh=finer, in_specs=in_specs, out_specs=out_specs, check_vma=False
    )
```

profile of v0, /device:TPU:24, one launch (start us, length us, event | category | flops | bytes accessed | tf_op | source)
XLA Modules:
  0.0 303.7 jit_solution(6002797034493604324)
XLA Ops:
  6.5 0.7 slice_bitcast_fusion
  7.3 0.6 pad_maximum_fusion
  7.9 0.0 all-gather.5.cloned.1.call-update
  7.9 0.0 all-gather.7.cloned.1.call-start
  8.0 0.7 fusion.40
  8.7 60.0 %all_gather.19 = bf16[64,256,16]{1,2,0:T(8,128)(2,1)} all-gather(bf16[1,256,16]{1,2,0:T(8,128)(2,1)S(1)} %get-tuple-element.13), channel_id=1, replica_groups=mesh['sp_0'=8,'sp_1'=8,'sp_2'=2,'tp'=4] {'sp_0','sp_1'}, dimensions={0}, use_global_device_ids=true | all-gather | bytes 532480 | tf_op jit(solution)/shard_map/all_gather | solution.py:49
  68.6 0.0 all-gather.7.cloned.1.call-update
  68.7 0.0 copy-start.4
  68.7 1.1 copy.36
  69.8 1.1 broadcast_in_dim.30
  70.9 4.3 %all-to-all-start = ((bf16[4,256,512]{1,2,0:T(8,128)(2,1)}), bf16[4,256,512]{1,2,0:T(8,128)(2,1)S(1)}, u32[]{:S(2)}, u32[]{:S(2)}) async-start(bf16[4,256,512]{1,2,0:T(8,128)(2,1)} %broadcast_in_dim.30), calls=%async_computation | async-start | bytes 2097152 | tf_op jit(solution)/shard_map/all_to_all | solution.py:20
  75.2 0.6 pad_maximum_fusion.1
  75.8 0.1 all-gather.9.cloned.1.call-update
  75.9 10.1 %all-to-all-done = bf16[4,256,512]{1,2,0:T(8,128)(2,1)S(1)} async-done(((bf16[4,256,512]{1,2,0:T(8,128)(2,1)}), bf16[4,256,512]{1,2,0:T(8,128)(2,1)S(1)}, u32[]{:S(2)}, u32[]{:S(2)}) %all-to-all-start) | async-done | bytes 1048608 | tf_op jit(solution)/shard_map/all_to_all | solution.py:20
  86.0 0.3 multiply_reduce_fusion.1
  86.4 0.3 fusion.3
  86.7 11.0 %all-gather.5.cloned.1.call-done = bf16[2048,512]{1,0:T(8,128)(2,1)} async-done(((bf16[16,512]{1,0:T(8,128)(2,1)}), bf16[2048,512]{1,0:T(8,128)(2,1)}) %all-gather.5.cloned.1.call-update) | async-done | bytes 2097168 | tf_op jit(solution)/shard_map/all_gather | solution.py:29
  97.7 1.8 fusion.18
  99.6 0.1 copy-done.2
  99.6 0.5 fusion.12
  100.2 2.1 collective-permute-start
  102.3 3.4 %collective-permute-done = bf16[128,256]{1,0:T(8,128)(2,1)S(1)} collective-permute-done((bf16[128,256]{1,0:T(8,128)(2,1)S(1)}, bf16[128,256]{1,0:T(8,128)(2,1)S(1)}, u32[]{:S(2)}, u32[]{:S(2)}) %collective-permute-start) | collective-permute-done | bytes 65568 | tf_op jit(solution)/shard_map/ppermute | solution.py:39
  105.8 0.0 copy-start.5
  105.8 4.8 %fusion.42 = (f32[256]{0:T(256)S(1)}, f32[1,256,256]{2,0,1:T(1,128)S(1)}) fusion(f32[1,128,256]{2,1,0:T(8,128)S(1)} %get-tuple-element.6, bf16[1,383,256]{2,1,0:T(8,128)(2,1)S(1)} %maximum_bitcast_fusion), kind=kOutput, calls=%fused_computation.76 | convolution fusion | flops 100728576 | bytes 590336 | tf_op jit(solution)/shard_map/conv_general_dilated | solution.py:90
  110.7 9.2 %all_to_all.40 = f32[4,256,1]{1,2,0:T(1,128)S(1)} all-to-all(f32[4,256,1]{1,2,0:T(1,128)S(1)} %broadcast_in_dim.32), channel_id=1, replica_groups=mesh['sp_0'=8,'sp_1'=8,'sp_2'=2,'tp'=4] {'tp'}, dimensions={0} | all-to-all | bytes 8192 | tf_op jit(solution)/shard_map/all_to_all | solution.py:20
  119.9 0.2 fusion.27
  120.1 0.6 broadcast_in_dim.33
  120.7 3.2 %all-to-all-start.2 = ((f32[4,256,1]{1,2,0:T(1,128)}), f32[4,256,1]{1,2,0:T(1,128)S(1)}, u32[]{:S(2)}, u32[]{:S(2)}) async-start(f32[4,256,1]{1,2,0:T(1,128)} %broadcast_in_dim.33), calls=%async_computation.2 | async-start | bytes 8192 | tf_op jit(solution)/shard_map/all_to_all | solution.py:20
  124.0 0.0 all-gather.11.cloned.1.call-start
  124.0 0.0 all-gather.7.cloned.1.call-done
  124.1 1.4 copy.40
  125.4 3.8 %all-to-all-done.2 = f32[4,256,1]{1,2,0:T(1,128)S(1)} async-done(((f32[4,256,1]{1,2,0:T(1,128)}), f32[4,256,1]{1,2,0:T(1,128)S(1)}, u32[]{:S(2)}, u32[]{:S(2)}) %all-to-all-start.2) | async-done | bytes 4128 | tf_op jit(solution)/shard_map/all_to_all | solution.py:20
  129.3 0.5 convolution_convert_fusion.1
  129.8 0.1 copy.83
  129.9 0.0 copy-start
  129.9 15.3 %all_to_all.41 = bf16[4,256,512]{2,1,0:T(8,128)(2,1)S(1)} all-to-all(bf16[4,256,512]{2,1,0:T(8,128)(2,1)S(1)} %bitcast.96), channel_id=1, replica_groups=mesh['sp_0'=8,'sp_1'=8,'sp_2'=2,'tp'=4] {'tp'}, dimensions={0} | all-to-all | bytes 2097152 | tf_op jit(solution)/shard_map/all_to_all | solution.py:68
  145.1 0.1 convert_reduce_fusion.1
  145.3 0.1 add_convert_fusion.1
  145.4 0.1 copy.42
  145.5 0.1 broadcast_in_dim.34
  145.6 14.3 %all_to_all.42 = bf16[4,256,512]{1,2,0:T(8,128)(2,1)S(1)} all-to-all(bf16[4,256,512]{1,2,0:T(8,128)(2,1)S(1)} %broadcast_in_dim.34), channel_id=1, replica_groups=mesh['sp_0'=8,'sp_1'=8,'sp_2'=2,'tp'=4] {'tp'}, dimensions={0} | all-to-all | bytes 2097152 | tf_op jit(solution)/shard_map/all_to_all | solution.py:20
  159.9 0.3 multiply_reduce_fusion
  160.2 0.3 fusion.1
  160.5 40.8 %all-gather.9.cloned.1.call-done = bf16[2048,512]{1,0:T(8,128)(2,1)} async-done(((bf16[16,512]{1,0:T(8,128)(2,1)}), bf16[2048,512]{1,0:T(8,128)(2,1)}) %all-gather.9.cloned.1.call-update) | async-done | bytes 2097168 | tf_op jit(solution)/shard_map/all_gather | solution.py:29
  201.3 1.8 fusion.15
  203.2 0.1 copy-done.1
  203.2 0.5 fusion.13
  203.7 2.1 collective-permute-start.1
  205.9 52.8 %all_gather.22 = bf16[64,256,16]{1,2,0:T(8,128)(2,1)} all-gather(bf16[1,256,16]{1,2,0:T(8,128)(2,1)S(1)} %get-tuple-element.14), channel_id=1, replica_groups=mesh['sp_0'=8,'sp_1'=8,'sp_2'=2,'tp'=4] {'sp_0','sp_1'}, dimensions={0}, use_global_device_ids=true | all-gather | bytes 532480 | tf_op jit(solution)/shard_map/all_gather | solution.py:49
  258.7 0.0 all-gather.11.cloned.1.call-update
  258.7 0.0 collective-permute-done.1
  258.8 4.8 %fusion.43 = (f32[256]{0:T(256)S(1)}, f32[1,256,256]{2,0,1:T(1,128)S(1)}) fusion(f32[1,128,256]{2,1,0:T(8,128)S(1)} %get-tuple-element.5, bf16[1,383,256]{2,1,0:T(8,128)(2,1)S(1)} %maximum_bitcast_fusion.1), kind=kOutput, calls=%fused_computation.77 | convolution fusion | flops 100728576 | bytes 590336 | tf_op jit(solution)/shard_map/conv_general_dilated | solution.py:90
  263.6 9.3 %all_to_all.43 = f32[4,256,1]{1,2,0:T(1,128)S(1)} all-to-all(f32[4,256,1]{1,2,0:T(1,128)S(1)} %broadcast_in_dim.36), channel_id=1, replica_groups=mesh['sp_0'=8,'sp_1'=8,'sp_2'=2,'tp'=4] {'tp'}, dimensions={0} | all-to-all | bytes 8192 | tf_op jit(solution)/shard_map/all_to_all | solution.py:20
  273.0 0.2 fusion.25
  273.2 0.6 broadcast_in_dim.37
  273.8 3.2 %all-to-all-start.6 = ((f32[4,256,1]{1,2,0:T(1,128)}), f32[4,256,1]{1,2,0:T(1,128)S(1)}, u32[]{:S(2)}, u32[]{:S(2)}) async-start(f32[4,256,1]{1,2,0:T(1,128)} %broadcast_in_dim.37), calls=%async_computation.6 | async-start | bytes 8192 | tf_op jit(solution)/shard_map/all_to_all | solution.py:20
  277.0 0.0 all-gather.11.cloned.1.call-done
  277.1 1.4 copy.46
  278.4 3.9 %all-to-all-done.6 = f32[4,256,1]{1,2,0:T(1,128)S(1)} async-done(((f32[4,256,1]{1,2,0:T(1,128)}), f32[4,256,1]{1,2,0:T(1,128)S(1)}, u32[]{:S(2)}, u32[]{:S(2)}) %all-to-all-start.6) | async-done | bytes 4128 | tf_op jit(solution)/shard_map/all_to_all | solution.py:20
  282.3 0.5 convolution_convert_fusion
  282.8 0.1 copy.82
  282.9 13.3 %all_to_all.44 = bf16[4,256,512]{2,1,0:T(8,128)(2,1)S(1)} all-to-all(bf16[4,256,512]{2,1,0:T(8,128)(2,1)S(1)} %bitcast.97), channel_id=1, replica_groups=mesh['sp_0'=8,'sp_1'=8,'sp_2'=2,'tp'=4] {'tp'}, dimensions={0} | all-to-all | bytes 2097152 | tf_op jit(solution)/shard_map/all_to_all | solution.py:68
  296.2 0.1 convert_reduce_fusion
  296.4 0.8 add_convert_fusion
  (30 shorter events, 0.3 us)
Async XLA Ops:
  6.5 91.2 %all-gather.5.cloned.1.call-start = ((), (), s32[]{:S(2)}) async-start(), calls=%async_computation.8 | async-start | bytes 2113536 | tf_op jit(solution)/shard_map/all_gather | solution.py:29
  7.9 116.1 %all-gather.7.cloned.1.call-start = ((), (), s32[]{:S(2)}) async-start(), calls=%async_computation.9 | async-start | bytes 1572864 | tf_op jit(solution)/shard_map/all_gather | solution.py:49
  68.7 7.2 %copy-start.4 = (f32[2,2048]{1,0:T(2,128)S(1)}, f32[2,2048]{1,0:T(2,128)}, u32[]{:S(2)}) copy-start(f32[2,2048]{1,0:T(2,128)} %param.8) | copy-start | bytes 49156
  70.9 15.2 %all-to-all-start = ((bf16[4,256,512]{1,2,0:T(8,128)(2,1)}), bf16[4,256,512]{1,2,0:T(8,128)(2,1)S(1)}, u32[]{:S(2)}, u32[]{:S(2)}) async-start(bf16[4,256,512]{1,2,0:T(8,128)(2,1)} %broadcast_in_dim.30), calls=%async_computation | async-start | bytes 2097152 | tf_op jit(solution)/shard_map/all_to_all | solution.py:20
  75.2 126.2 %all-gather.9.cloned.1.call-start = ((), (), s32[]{:S(2)}) async-start(), calls=%async_computation.10 | async-start | bytes 2113536 | tf_op jit(solution)/shard_map/all_gather | solution.py:29
  97.7 1.9 copy-start.2
  99.6 2.7 copy-start.3
  100.2 5.6 %collective-permute-start = (bf16[128,256]{1,0:T(8,128)(2,1)S(1)}, bf16[128,256]{1,0:T(8,128)(2,1)S(1)}, u32[]{:S(2)}, u32[]{:S(2)}) collective-permute-start(bf16[128,256]{1,0:T(8,128)(2,1)S(1)} %slice.82), channel_id=1, source_target_pairs={{0,4},{4,8},{8,12},{12,16},{16,20},{20,24},{24,28},{28,32},{32,36}... | collective-permute-start | bytes 196616 | tf_op jit(solution)/shard_map/ppermute | solution.py:39
  105.8 18.2 %copy-start.5 = (f32[2,256]{1,0:T(2,128)S(1)}, f32[2,256]{1,0:T(2,128)}, u32[]{:S(2)}) copy-start(f32[2,256]{1,0:T(2,128)} %param.12) | copy-start | bytes 6148
  120.7 8.5 %all-to-all-start.2 = ((f32[4,256,1]{1,2,0:T(1,128)}), f32[4,256,1]{1,2,0:T(1,128)S(1)}, u32[]{:S(2)}, u32[]{:S(2)}) async-start(f32[4,256,1]{1,2,0:T(1,128)} %broadcast_in_dim.33), calls=%async_computation.2 | async-start | bytes 8192 | tf_op jit(solution)/shard_map/all_to_all | solution.py:20
  124.0 153.1 %all-gather.11.cloned.1.call-start = ((), (), s32[]{:S(2)}) async-start(), calls=%async_computation.11 | async-start | bytes 1572864 | tf_op jit(solution)/shard_map/all_gather | solution.py:49
  129.9 15.4 %copy-start = (bf16[256,512]{1,0:T(8,128)(2,1)S(1)}, bf16[256,512]{1,0:T(8,128)(2,1)}, u32[]{:S(2)}) copy-start(bf16[256,512]{1,0:T(8,128)(2,1)} %param.7) | copy-start | bytes 786436
  201.3 1.9 copy-start.1
  203.7 54.9 %collective-permute-start.1 = (bf16[128,256]{1,0:T(8,128)(2,1)S(1)}, bf16[128,256]{1,0:T(8,128)(2,1)S(1)}, u32[]{:S(2)}, u32[]{:S(2)}) collective-permute-start(bf16[128,256]{1,0:T(8,128)(2,1)S(1)} %slice.86), channel_id=1, source_target_pairs={{0,4},{4,8},{8,12},{12,16},{16,20},{20,24},{24,28},{28,32},{32,36}... | collective-permute-start | bytes 196616 | tf_op jit(solution)/shard_map/ppermute | solution.py:39
  273.8 8.5 %all-to-all-start.6 = ((f32[4,256,1]{1,2,0:T(1,128)}), f32[4,256,1]{1,2,0:T(1,128)S(1)}, u32[]{:S(2)}, u32[]{:S(2)}) async-start(f32[4,256,1]{1,2,0:T(1,128)} %broadcast_in_dim.37), calls=%async_computation.6 | async-start | bytes 8192 | tf_op jit(solution)/shard_map/all_to_all | solution.py:20
Sparse Core Ops, SparseCore 0:
  10.5 87.2 all-gather.4
  99.8 14.3 all-gather.6
  117.3 83.9 all-gather.8
  258.8 14.8 all-gather.10
where the time goes:
time: 304 us
  blocking collectives  174 us (57%)
  waiting for transfers between devices  73.2 us (24%)
  matrix products  15.4 us (5%)
  starting transfers between devices  15.1 us (5%)
  between operations  13.4 us (4%)
  local copies, waits for them, and re-layouts  8.17 us (3%)
  other arithmetic  4.21 us (1%)
    all_gather x2, blocking collectives, stacked_from(): parts = lax.all_gather(parts, axes[k], axis=0, tiled=True)  113 us
    all_gather x2, waiting for transfers between devices, in_one_piece(): whole, at, done = (lax.all_gather(both, axis, axis=dim, tiled=True), 0, [])  51.8 us
    all_to_all x3, blocking collectives, sent_to_all(): return lax.all_to_all(copies, axis, split_axis=0, concat_axis=0, tiled=True)  32.8 us
    all_to_all x2, blocking collectives, sum_at_owner(): lax.all_to_all(parts, axis, split_axis=0, concat_axis=0, tiled=True)  28.6 us
    all_to_all x3, waiting for transfers between devices, sent_to_all(): return lax.all_to_all(copies, axis, split_axis=0, concat_axis=0, tiled=True)  17.8 us
    all_to_all x3, starting transfers between devices, sent_to_all(): return lax.all_to_all(copies, axis, split_axis=0, concat_axis=0, tiled=True)  10.8 us
    conv_general_dilated x2, matrix products, shards(): lax.conv_general_dilated(padded[None], conv_taps[layer][:, None, :], (1,)...  9.67 us
  transfers between devices with their start and end apart: 9, of which 6 were waited for; matrix products, arithmetic and copies ran while one was open for 7% of the time, Pallas kernels for 0%

commit v1 on v0

--- a/solution.py
+++ b/solution.py
@@ -3,6 +3,7 @@
 from jax import lax
 from jax.sharding import Mesh
 from jax.sharding import PartitionSpec as P
+from jax.lax import all_to_all, psum
 
 C = 1024
 LAYERS = 2
@@ -46,7 +47,8 @@
 def stacked_from(shard, axes, turns):
     parts = shard[None]
     for k in turns:
-        parts = lax.all_gather(parts, axes[k], axis=0, tiled=True)
+        base_x = axes[k]
+        parts = jnp.concatenate(all_to_all(jnp.stack(psum(1, base_x) * [parts]), base_x, 0, 0), 0)
     held = [lax.axis_size(axes[k]) for k in reversed(turns)]
     parts = parts.reshape(*held, *shard.shape)
     turned = sorted(range(len(turns)), key=lambda place: turns[len(turns) - 1 - place])

time: 304 us -> 252 us (0.83)
  the two profiles are of different devices: /device:TPU:24 before, /device:TPU:8 now
where the time goes in v1:
time: 252 us; the launch traced here: 251 us
  waiting for transfers between devices  100 us (40%)
  starting transfers between devices  57 us (23%)
  blocking collectives  49.9 us (20%)
  matrix products  15.4 us (6%)
  between operations  13.8 us (5%)
  local copies, waits for them, and re-layouts  7.83 us (3%)
  other arithmetic  6.34 us (3%)
    all_gather x2, waiting for transfers between devices, in_one_piece(): whole, at, done = (lax.all_gather(both, axis, axis=dim, tiled=True), 0, [])  53.6 us
    all_to_all x4, starting transfers between devices, stacked_from(): all_to_all(jnp.stack(psum(1, base_x) * [parts]), base_x, 0, 0)  34.5 us
    all_to_all x2, blocking collectives, sum_at_owner(): lax.all_to_all(parts, axis, split_axis=0, concat_axis=0, tiled=True)  34 us
    all_to_all x5, waiting for transfers between devices, sent_to_all(): return lax.all_to_all(copies, axis, split_axis=0, concat_axis=0, tiled=True)  32.9 us
    all_to_all x5, starting transfers between devices, sent_to_all(): return lax.all_to_all(copies, axis, split_axis=0, concat_axis=0, tiled=True)  18.3 us
    all_to_all x1, blocking collectives, sent_to_all(): return lax.all_to_all(copies, axis, split_axis=0, concat_axis=0, tiled=True)  15.8 us
    conv_general_dilated x2, matrix products, shards(): lax.conv_general_dilated(padded[None], conv_taps[layer][:, None, :], (1,)...  9.67 us
    ppermute x2, waiting for transfers between devices, from_behind(): lax.ppermute(value, axis, [(source, source + steps) for source in range(i...  7.5 us
  transfers between devices with their start and end apart: 13, of which 11 were waited for; matrix products, arithmetic and copies ran while one was open for 10% of the time, Pallas kernels for 0%

profile of v1, /device:TPU:8, one launch (start us, length us, event | category | flops | bytes accessed | tf_op | source)
XLA Modules:
  0.0 250.6 jit_solution(16076256389904985067)
XLA Ops:
  6.5 0.8 slice_bitcast_fusion.1
  7.3 0.6 pad_maximum_fusion.2
  7.9 1.1 copy.30
  9.0 1.1 broadcast_in_dim.30
  10.1 4.3 %all-to-all-start = ((bf16[4,256,512]{1,2,0:T(8,128)(2,1)}), bf16[4,256,512]{1,2,0:T(8,128)(2,1)S(1)}, u32[]{:S(2)}, u32[]{:S(2)}) async-start(bf16[4,256,512]{1,2,0:T(8,128)(2,1)} %broadcast_in_dim.30), calls=%async_computation | async-start | bytes 2097152 | tf_op jit(solution)/shard_map/all_to_all | solution.py:21
  14.4 0.6 pad_maximum_fusion.3
  15.0 0.1 all-gather.5.cloned.1.call-update
  15.2 14.3 %all-to-all-done = bf16[4,256,512]{1,2,0:T(8,128)(2,1)S(1)} async-done(((bf16[4,256,512]{1,2,0:T(8,128)(2,1)}), bf16[4,256,512]{1,2,0:T(8,128)(2,1)S(1)}, u32[]{:S(2)}, u32[]{:S(2)}) %all-to-all-start) | async-done | bytes 1048608 | tf_op jit(solution)/shard_map/all_to_all | solution.py:21
  29.5 0.9 stack.12
  30.3 16.6 %all-to-all-start.3 = ((bf16[64,1,256,16]{2,3,1,0:T(8,128)(2,1)}), bf16[64,1,256,16]{2,3,1,0:T(8,128)(2,1)S(1)}, u32[]{:S(2)}, u32[]{:S(2)}) async-start(bf16[64,1,256,16]{2,3,1,0:T(8,128)(2,1)} %stack.12), calls=%async_computation.3 | async-start | bytes 1048576 | tf_op jit(solution)/shard_map/all_to_all | solution.py:51
  46.9 0.3 multiply_reduce_fusion.1
  47.2 0.3 fusion.3
  47.6 53.6 %all-gather.3.cloned.1.call-done = bf16[2048,512]{1,0:T(8,128)(2,1)} async-done(((bf16[16,512]{1,0:T(8,128)(2,1)}), bf16[2048,512]{1,0:T(8,128)(2,1)}) %all-gather.3.cloned.1.call-update) | async-done | bytes 2097168 | tf_op jit(solution)/shard_map/all_gather | solution.py:30
  101.2 1.8 fusion.18
  103.0 0.1 copy-done.2
  103.1 0.5 fusion.12
  103.6 2.1 collective-permute-start
  105.8 3.4 %collective-permute-done = bf16[128,256]{1,0:T(8,128)(2,1)S(1)} collective-permute-done((bf16[128,256]{1,0:T(8,128)(2,1)S(1)}, bf16[128,256]{1,0:T(8,128)(2,1)S(1)}, u32[]{:S(2)}, u32[]{:S(2)}) %collective-permute-start) | collective-permute-done | bytes 65568 | tf_op jit(solution)/shard_map/ppermute | solution.py:40
  109.2 4.8 %fusion.41 = (f32[256]{0:T(256)S(1)}, f32[1,256,256]{2,0,1:T(1,128)S(1)}) fusion(f32[1,128,256]{2,1,0:T(8,128)S(1)} %get-tuple-element.6, bf16[1,383,256]{2,1,0:T(8,128)(2,1)S(1)} %maximum_bitcast_fusion), kind=kOutput, calls=%fused_computation.79 | convolution fusion | flops 100728576 | bytes 590336 | tf_op jit(solution)/shard_map/conv_general_dilated | solution.py:92
  114.1 0.6 broadcast_in_dim.32
  114.7 4.2 %all-to-all-start.1 = ((f32[4,256,1]{1,2,0:T(1,128)}), f32[4,256,1]{1,2,0:T(1,128)S(1)}, u32[]{:S(2)}, u32[]{:S(2)}) async-start(f32[4,256,1]{1,2,0:T(1,128)} %broadcast_in_dim.32), calls=%async_computation.1 | async-start | bytes 8192 | tf_op jit(solution)/shard_map/all_to_all | solution.py:21
  118.9 1.1 pad_maximum_fusion
  120.0 4.2 %all-to-all-done.1 = f32[4,256,1]{1,2,0:T(1,128)S(1)} async-done(((f32[4,256,1]{1,2,0:T(1,128)}), f32[4,256,1]{1,2,0:T(1,128)S(1)}, u32[]{:S(2)}, u32[]{:S(2)}) %all-to-all-start.1) | async-done | bytes 4128 | tf_op jit(solution)/shard_map/all_to_all | solution.py:21
  124.2 3.6 %all-to-all-start.4 = ((bf16[2,64,256,16]{2,3,1,0:T(8,128)(2,1)}), bf16[2,64,256,16]{2,3,1,0:T(8,128)(2,1)S(1)}, u32[]{:S(2)}, u32[]{:S(2)}) async-start(bf16[2,64,256,16]{2,3,1,0:T(8,128)(2,1)} %pad_maximum_fusion), calls=%async_computation.4 | async-start | bytes 2097152 | tf_op jit(solution)/shard_map/all_to_all | solution.py:51
  127.9 0.2 fusion.27
  128.0 1.9 all-to-all-done.4
  129.9 0.6 broadcast_in_dim.33
  130.5 3.2 %all-to-all-start.2 = ((f32[4,256,1]{1,2,0:T(1,128)}), f32[4,256,1]{1,2,0:T(1,128)S(1)}, u32[]{:S(2)}, u32[]{:S(2)}) async-start(f32[4,256,1]{1,2,0:T(1,128)} %broadcast_in_dim.33), calls=%async_computation.2 | async-start | bytes 8192 | tf_op jit(solution)/shard_map/all_to_all | solution.py:21
  133.8 0.1 copy.34
  133.9 5.1 %all-to-all-done.2 = f32[4,256,1]{1,2,0:T(1,128)S(1)} async-done(((f32[4,256,1]{1,2,0:T(1,128)}), f32[4,256,1]{1,2,0:T(1,128)S(1)}, u32[]{:S(2)}, u32[]{:S(2)}) %all-to-all-start.2) | async-done | bytes 4128 | tf_op jit(solution)/shard_map/all_to_all | solution.py:21
  139.1 0.5 convolution_convert_fusion.1
  139.6 0.1 copy.77
  139.7 17.1 %all_to_all.60 = bf16[4,256,512]{2,1,0:T(8,128)(2,1)S(1)} all-to-all(bf16[4,256,512]{2,1,0:T(8,128)(2,1)S(1)} %bitcast.100), channel_id=1, replica_groups=mesh['sp_0'=8,'sp_1'=8,'sp_2'=2,'tp'=4] {'tp'}, dimensions={0} | all-to-all | bytes 2097152 | tf_op jit(solution)/shard_map/all_to_all | solution.py:70
  156.8 0.1 convert_reduce_fusion.1
  156.9 0.1 add_convert_fusion.1
  157.0 0.1 copy.36
  157.1 0.1 broadcast_in_dim.34
  157.2 15.8 %all_to_all.61 = bf16[4,256,512]{1,2,0:T(8,128)(2,1)S(1)} all-to-all(bf16[4,256,512]{1,2,0:T(8,128)(2,1)S(1)} %broadcast_in_dim.34), channel_id=1, replica_groups=mesh['sp_0'=8,'sp_1'=8,'sp_2'=2,'tp'=4] {'tp'}, dimensions={0} | all-to-all | bytes 2097152 | tf_op jit(solution)/shard_map/all_to_all | solution.py:21
  173.1 0.8 stack.14
  173.9 10.7 %all-to-all-start.9 = ((bf16[64,1,256,16]{2,3,1,0:T(8,128)(2,1)}), bf16[64,1,256,16]{2,3,1,0:T(8,128)(2,1)S(1)}, u32[]{:S(2)}, u32[]{:S(2)}) async-start(bf16[64,1,256,16]{2,3,1,0:T(8,128)(2,1)} %stack.14), calls=%async_computation.9 | async-start | bytes 1048576 | tf_op jit(solution)/shard_map/all_to_all | solution.py:51
  184.6 0.3 multiply_reduce_fusion
  184.9 0.3 fusion.1
  185.3 1.8 fusion.15
  187.2 0.5 fusion.13
  187.7 2.1 collective-permute-start.1
  189.9 4.1 %collective-permute-done.1 = bf16[128,256]{1,0:T(8,128)(2,1)S(1)} collective-permute-done((bf16[128,256]{1,0:T(8,128)(2,1)S(1)}, bf16[128,256]{1,0:T(8,128)(2,1)S(1)}, u32[]{:S(2)}, u32[]{:S(2)}) %collective-permute-start.1) | collective-permute-done | bytes 65568 | tf_op jit(solution)/shard_map/ppermute | solution.py:40
  194.0 4.8 %fusion.42 = (f32[256]{0:T(256)S(1)}, f32[1,256,256]{2,0,1:T(1,128)S(1)}) fusion(f32[1,128,256]{2,1,0:T(8,128)S(1)} %get-tuple-element.5, bf16[1,383,256]{2,1,0:T(8,128)(2,1)S(1)} %maximum_bitcast_fusion.1), kind=kOutput, calls=%fused_computation.80 | convolution fusion | flops 100728576 | bytes 590336 | tf_op jit(solution)/shard_map/conv_general_dilated | solution.py:92
  198.8 2.5 %all-to-all-done.9 = bf16[64,1,256,16]{2,3,1,0:T(8,128)(2,1)S(1)} async-done(((bf16[64,1,256,16]{2,3,1,0:T(8,128)(2,1)}), bf16[64,1,256,16]{2,3,1,0:T(8,128)(2,1)S(1)}, u32[]{:S(2)}, u32[]{:S(2)}) %all-to-all-start.9) | async-done | bytes 524320 | tf_op jit(solution)/shard_map/all_to_all | solution.py:51
  201.4 0.6 broadcast_in_dim.36
  201.9 3.2 %all-to-all-start.7 = ((f32[4,256,1]{1,2,0:T(1,128)}), f32[4,256,1]{1,2,0:T(1,128)S(1)}, u32[]{:S(2)}, u32[]{:S(2)}) async-start(f32[4,256,1]{1,2,0:T(1,128)} %broadcast_in_dim.36), calls=%async_computation.7 | async-start | bytes 8192 | tf_op jit(solution)/shard_map/all_to_all | solution.py:21
  205.2 1.1 pad_maximum_fusion.1
  206.3 4.2 %all-to-all-done.7 = f32[4,256,1]{1,2,0:T(1,128)S(1)} async-done(((f32[4,256,1]{1,2,0:T(1,128)}), f32[4,256,1]{1,2,0:T(1,128)S(1)}, u32[]{:S(2)}, u32[]{:S(2)}) %all-to-all-start.7) | async-done | bytes 4128 | tf_op jit(solution)/shard_map/all_to_all | solution.py:21
  210.5 3.6 %all-to-all-start.10 = ((bf16[2,64,256,16]{2,3,1,0:T(8,128)(2,1)}), bf16[2,64,256,16]{2,3,1,0:T(8,128)(2,1)S(1)}, u32[]{:S(2)}, u32[]{:S(2)}) async-start(bf16[2,64,256,16]{2,3,1,0:T(8,128)(2,1)} %pad_maximum_fusion.1), calls=%async_computation.10 | async-start | bytes 2097152 | tf_op jit(solution)/shard_map/all_to_all | solution.py:51
  214.1 0.2 fusion.25
  214.3 1.9 all-to-all-done.10
  216.2 0.6 broadcast_in_dim.37
  216.7 3.2 %all-to-all-start.8 = ((f32[4,256,1]{1,2,0:T(1,128)}), f32[4,256,1]{1,2,0:T(1,128)S(1)}, u32[]{:S(2)}, u32[]{:S(2)}) async-start(f32[4,256,1]{1,2,0:T(1,128)} %broadcast_in_dim.37), calls=%async_computation.8 | async-start | bytes 8192 | tf_op jit(solution)/shard_map/all_to_all | solution.py:21
  220.0 0.1 copy.40
  220.1 5.1 %all-to-all-done.8 = f32[4,256,1]{1,2,0:T(1,128)S(1)} async-done(((f32[4,256,1]{1,2,0:T(1,128)}), f32[4,256,1]{1,2,0:T(1,128)S(1)}, u32[]{:S(2)}, u32[]{:S(2)}) %all-to-all-start.8) | async-done | bytes 4128 | tf_op jit(solution)/shard_map/all_to_all | solution.py:21
  225.3 0.5 convolution_convert_fusion
  225.8 0.1 copy.76
  225.9 16.9 %all_to_all.62 = bf16[4,256,512]{2,1,0:T(8,128)(2,1)S(1)} all-to-all(bf16[4,256,512]{2,1,0:T(8,128)(2,1)S(1)} %bitcast.101), channel_id=1, replica_groups=mesh['sp_0'=8,'sp_1'=8,'sp_2'=2,'tp'=4] {'tp'}, dimensions={0} | all-to-all | bytes 2097152 | tf_op jit(solution)/shard_map/all_to_all | solution.py:70
  242.9 0.1 convert_reduce_fusion
  243.0 0.8 add_convert_fusion
  (38 shorter events, 0.4 us)
Async XLA Ops:
  6.5 8.6 %copy-start.4 = (bf16[2,256,16]{1,2,0:T(8,128)(2,1)S(1)}, bf16[2,256,16]{1,2,0:T(8,128)(2,1)}, u32[]{:S(2)}) copy-start(bf16[2,256,16]{1,2,0:T(8,128)(2,1)} %param.13) | copy-start | bytes 49156
  6.5 8.6 %copy-start.5 = (f32[2,2048]{1,0:T(2,128)S(1)}, f32[2,2048]{1,0:T(2,128)}, u32[]{:S(2)}) copy-start(f32[2,2048]{1,0:T(2,128)} %param.8) | copy-start | bytes 49156
  6.5 94.6 %all-gather.3.cloned.1.call-start = ((), (), s32[]{:S(2)}) async-start(), calls=%async_computation.12 | async-start | bytes 2113536 | tf_op jit(solution)/shard_map/all_gather | solution.py:30
  10.1 19.4 %all-to-all-start = ((bf16[4,256,512]{1,2,0:T(8,128)(2,1)}), bf16[4,256,512]{1,2,0:T(8,128)(2,1)S(1)}, u32[]{:S(2)}, u32[]{:S(2)}) async-start(bf16[4,256,512]{1,2,0:T(8,128)(2,1)} %broadcast_in_dim.30), calls=%async_computation | async-start | bytes 2097152 | tf_op jit(solution)/shard_map/all_to_all | solution.py:21
  14.4 170.9 %all-gather.5.cloned.1.call-start = ((), (), s32[]{:S(2)}) async-start(), calls=%async_computation.13 | async-start | bytes 2113536 | tf_op jit(solution)/shard_map/all_gather | solution.py:30
  30.3 83.8 %all-to-all-start.3 = ((bf16[64,1,256,16]{2,3,1,0:T(8,128)(2,1)}), bf16[64,1,256,16]{2,3,1,0:T(8,128)(2,1)S(1)}, u32[]{:S(2)}, u32[]{:S(2)}) async-start(bf16[64,1,256,16]{2,3,1,0:T(8,128)(2,1)} %stack.12), calls=%async_computation.3 | async-start | bytes 1048576 | tf_op jit(solution)/shard_map/all_to_all | solution.py:51
  101.2 1.9 copy-start.2
  103.1 2.7 %copy-start.3 = (f32[2,128,256]{2,1,0:T(8,128)S(1)}, f32[2,128,256]{2,1,0:T(8,128)}, u32[]{:S(2)}) copy-start(f32[2,128,256]{2,1,0:T(8,128)} %param.11) | copy-start | bytes 786436
  103.6 5.6 %collective-permute-start = (bf16[128,256]{1,0:T(8,128)(2,1)S(1)}, bf16[128,256]{1,0:T(8,128)(2,1)S(1)}, u32[]{:S(2)}, u32[]{:S(2)}) collective-permute-start(bf16[128,256]{1,0:T(8,128)(2,1)S(1)} %slice.88), channel_id=1, source_target_pairs={{0,4},{4,8},{8,12},{12,16},{16,20},{20,24},{24,28},{28,32},{32,36}... | collective-permute-start | bytes 196616 | tf_op jit(solution)/shard_map/ppermute | solution.py:40
  114.1 19.7 %copy-start.6 = (f32[2,256]{1,0:T(2,128)S(1)}, f32[2,256]{1,0:T(2,128)}, u32[]{:S(2)}) copy-start(f32[2,256]{1,0:T(2,128)} %param.12) | copy-start | bytes 6148
  114.7 9.5 %all-to-all-start.1 = ((f32[4,256,1]{1,2,0:T(1,128)}), f32[4,256,1]{1,2,0:T(1,128)S(1)}, u32[]{:S(2)}, u32[]{:S(2)}) async-start(f32[4,256,1]{1,2,0:T(1,128)} %broadcast_in_dim.32), calls=%async_computation.1 | async-start | bytes 8192 | tf_op jit(solution)/shard_map/all_to_all | solution.py:21
  124.2 5.7 %all-to-all-start.4 = ((bf16[2,64,256,16]{2,3,1,0:T(8,128)(2,1)}), bf16[2,64,256,16]{2,3,1,0:T(8,128)(2,1)S(1)}, u32[]{:S(2)}, u32[]{:S(2)}) async-start(bf16[2,64,256,16]{2,3,1,0:T(8,128)(2,1)} %pad_maximum_fusion), calls=%async_computation.4 | async-start | bytes 2097152 | tf_op jit(solution)/shard_map/all_to_all | solution.py:51
  130.5 8.5 %all-to-all-start.2 = ((f32[4,256,1]{1,2,0:T(1,128)}), f32[4,256,1]{1,2,0:T(1,128)S(1)}, u32[]{:S(2)}, u32[]{:S(2)}) async-start(f32[4,256,1]{1,2,0:T(1,128)} %broadcast_in_dim.33), calls=%async_computation.2 | async-start | bytes 8192 | tf_op jit(solution)/shard_map/all_to_all | solution.py:21
  139.7 17.2 %copy-start = (bf16[256,512]{1,0:T(8,128)(2,1)S(1)}, bf16[256,512]{1,0:T(8,128)(2,1)}, u32[]{:S(2)}) copy-start(bf16[256,512]{1,0:T(8,128)(2,1)} %param.7) | copy-start | bytes 786436
  173.9 27.5 %all-to-all-start.9 = ((bf16[64,1,256,16]{2,3,1,0:T(8,128)(2,1)}), bf16[64,1,256,16]{2,3,1,0:T(8,128)(2,1)S(1)}, u32[]{:S(2)}, u32[]{:S(2)}) async-start(bf16[64,1,256,16]{2,3,1,0:T(8,128)(2,1)} %stack.14), calls=%async_computation.9 | async-start | bytes 1048576 | tf_op jit(solution)/shard_map/all_to_all | solution.py:51
  185.3 1.9 copy-start.1
  187.7 6.2 %collective-permute-start.1 = (bf16[128,256]{1,0:T(8,128)(2,1)S(1)}, bf16[128,256]{1,0:T(8,128)(2,1)S(1)}, u32[]{:S(2)}, u32[]{:S(2)}) collective-permute-start(bf16[128,256]{1,0:T(8,128)(2,1)S(1)} %slice.92), channel_id=1, source_target_pairs={{0,4},{4,8},{8,12},{12,16},{16,20},{20,24},{24,28},{28,32},{32,36}... | collective-permute-start | bytes 196616 | tf_op jit(solution)/shard_map/ppermute | solution.py:40
  201.9 8.5 %all-to-all-start.7 = ((f32[4,256,1]{1,2,0:T(1,128)}), f32[4,256,1]{1,2,0:T(1,128)S(1)}, u32[]{:S(2)}, u32[]{:S(2)}) async-start(f32[4,256,1]{1,2,0:T(1,128)} %broadcast_in_dim.36), calls=%async_computation.7 | async-start | bytes 8192 | tf_op jit(solution)/shard_map/all_to_all | solution.py:21
  210.5 5.7 %all-to-all-start.10 = ((bf16[2,64,256,16]{2,3,1,0:T(8,128)(2,1)}), bf16[2,64,256,16]{2,3,1,0:T(8,128)(2,1)S(1)}, u32[]{:S(2)}, u32[]{:S(2)}) async-start(bf16[2,64,256,16]{2,3,1,0:T(8,128)(2,1)} %pad_maximum_fusion.1), calls=%async_computation.10 | async-start | bytes 2097152 | tf_op jit(solution)/shard_map/all_to_all | solution.py:51
  216.7 8.5 %all-to-all-start.8 = ((f32[4,256,1]{1,2,0:T(1,128)}), f32[4,256,1]{1,2,0:T(1,128)S(1)}, u32[]{:S(2)}, u32[]{:S(2)}) async-start(f32[4,256,1]{1,2,0:T(1,128)} %broadcast_in_dim.37), calls=%async_computation.8 | async-start | bytes 8192 | tf_op jit(solution)/shard_map/all_to_all | solution.py:21
Sparse Core Ops, SparseCore 0:
  10.5 90.6 all-gather.2
  104.3 80.0 all-gather.4
